TPU v7x, 32 devices: a whole 2x2x4 slice. The times are simulated.
32 devices in a mesh: grp: 2 (over y), sp: 4 (over z), tp: 4 (over x, core).
Axes of the slice: x: 2, y: 2, z: 4, core: 2. Of those that a mesh axis runs over, the one named last changes fastest.
Arguments:
- queries_small: bfloat16 [2048, 1024], P(('grp', 'sp'), 'tp'), parts along dimension 0, may hold values from -6 to 6
- keys_small: bfloat16 [2048, 512], P(('grp', 'sp'), 'tp'), parts along dimension 0, may hold values from -6 to 6
- values_small: bfloat16 [2048, 512], P(('grp', 'sp'), 'tp'), parts along dimension 0, may hold values from -6 to 6
- queries_large: bfloat16 [2048, 1024], P(('grp', 'sp'), 'tp'), parts along dimension 0, may hold values from -6 to 6
- keys_large: bfloat16 [2048, 512], P(('grp', 'sp'), 'tp'), parts along dimension 0, may hold values from -6 to 6
- values_large: bfloat16 [2048, 512], P(('grp', 'sp'), 'tp'), parts along dimension 0, may hold values from -6 to 6
- query_gain_small: float32 [128], P('grp'), parts along dimension 0, may hold values from 1.2 to 12
- key_gain_small: float32 [128], P('grp'), parts along dimension 0, may hold values from 1.2 to 12
- query_gain_large: float32 [256], P('grp'), parts along dimension 0, may hold values from 1.2 to 12
- key_gain_large: float32 [256], P('grp'), parts along dimension 0, may hold values from 1.2 to 12
- residual_in: bfloat16 [2048, 2048], P(('grp', 'sp', 'tp')), parts along dimension 0, may hold values from -1.5 to 1.5
- out_weight_small: bfloat16 [1024, 2048], P('tp'), may hold values from -0.125 to 0.125
- out_weight_large: bfloat16 [1024, 2048], P('tp'), may hold values from -0.125 to 0.125
- norm_gain: float32 [2048], replicated, may hold values from 0.1 to 1.9
- routes: int32 [2048, 2], P(('grp', 'sp', 'tp')), parts along dimension 0, may hold values from 0 to 7, all different within a row; in each aligned block of 64 rows (0 to 63, 64 to 127, ...) at most 32 rows name the same one
- route_scores: float32 [2048, 2], P(('grp', 'sp', 'tp')), parts along dimension 0, may hold values from 0.05 to 1
- expert_gate: bfloat16 [8, 2048, 1024], P('sp', None, 'tp'), may hold values from -0.125 to 0.125
- expert_up: bfloat16 [8, 2048, 1024], P('sp', None, 'tp'), may hold values from -0.125 to 0.125
- expert_down: bfloat16 [8, 1024, 2048], P('sp', 'tp'), may hold values from -0.1875 to 0.1875
Outputs:
- result: bfloat16 [2048, 2048], P(('grp', 'sp', 'tp')), parts along dimension 0
There are 2 independent parts, one for each index of `grp`. A program takes and returns all parts, laid end to end along the dimension named above; an argument that names none is the same for every part. Nothing has to cross between parts.
Inputs may be any that keep to these rules, and one draw needn't show every extreme that they name: `routes`: each token names 2 different experts; within the rows of one device (aligned blocks of 64 tokens) no expert is named more than 32 times, a bound that some block reaches.
All inputs are finite; a program needn't handle non-finite values.
Results may differ from a plain program's by a relative error of at most 0.02.
The roundings to bfloat16 on the way count: a program that leaves them out, or rounds other values in their place, can miss the bound.
Values may be sent and summed in bfloat16 or wider, within the bound.
A program may use at most 128 MiB of HBM per device.

v0:
```python
import jax
import jax.numpy as jnp
from jax import lax
from jax.sharding import PartitionSpec as P

HS_SMALL = 64
HS_LARGE = 128
GRID_W = 64
theta_base = 10000.0
norm_eps = 1e-06
block_target = 1280


def grid_tables(offset, length, head_size):
    places = offset + jnp.arange(length, dtype=jnp.int32)
    grid_rows = (places // GRID_W).astype(jnp.float32)
    grid_cols = (places % GRID_W).astype(jnp.float32)
    rates = jnp.power(
        theta_base, -2.0 * jnp.arange(head_size // 4, dtype=jnp.float32) / (head_size // 2)
    )
    row_angles = grid_rows[:, None, None] * rates
    col_angles = grid_cols[:, None, None] * rates
    return (jnp.cos(row_angles), jnp.sin(row_angles), jnp.cos(col_angles), jnp.sin(col_angles))


def half_turn(segment, cosine, sine_part):
    half_size = segment.shape[-1] // 2
    leading = segment[..., :half_size]
    trailing = segment[..., half_size:]
    return jnp.concatenate(
        [leading * cosine - trailing * sine_part, trailing * cosine + leading * sine_part], axis=-1
    )


def grid_turn(vectors, tables):
    row_cos, row_sin, col_cos, col_sin = tables
    half_size = vectors.shape[-1] // 2
    return jnp.concatenate(
        [
            half_turn(vectors[..., :half_size], row_cos, row_sin),
            half_turn(vectors[..., half_size:], col_cos, col_sin),
        ],
        axis=-1,
    )


def normed_turn(raw_rows, gain, tables):
    widened = raw_rows.astype(jnp.float32)
    scaled = (
        widened * lax.rsqrt(jnp.mean(widened * widened, axis=-1, keepdims=True) + norm_eps) * gain
    )
    return grid_turn(scaled, tables).astype(jnp.bfloat16)


def block_rows(row_count, shard_rows):
    shards = row_count // shard_rows
    chosen = 1
    for factor in range(1, max(1, block_target // shard_rows) + 1):
        if shards % factor == 0:
            chosen = factor
    return chosen * shard_rows


def attend_block(state, queries, key_rows, value_rows):
    largest, weight_sum, accumulated = state
    head_size = queries.shape[-1]
    kv_local = queries.shape[1]
    key_heads = key_rows.reshape(key_rows.shape[0], kv_local, head_size)
    value_heads = value_rows.reshape(value_rows.shape[0], kv_local, head_size)
    scores = jnp.einsum(
        "qgrd,kgd->qgrk", queries, key_heads, preferred_element_type=jnp.float32
    ) * head_size ** (-0.5)
    peak_score = jnp.maximum(largest, jnp.max(scores, axis=-1))
    shrink = jnp.exp(largest - peak_score)
    weights = jnp.exp(scores - peak_score[..., None])
    weight_sum = weight_sum * shrink + jnp.sum(weights, axis=-1)
    accumulated = accumulated * shrink[..., None] + jnp.einsum(
        "qgrk,kgd->qgrd",
        weights.astype(jnp.bfloat16),
        value_heads,
        preferred_element_type=jnp.float32,
    )
    return (peak_score, weight_sum, accumulated)


def attend_rows(state, queries, key_rows, value_rows):
    row_count = key_rows.shape[0]
    step_rows = block_rows(row_count, queries.shape[0])
    if step_rows == row_count:
        return attend_block(state, queries, key_rows, value_rows)

    def one_block(block_index, carried):
        offset = block_index * step_rows
        return attend_block(
            carried,
            queries,
            lax.dynamic_slice_in_dim(key_rows, offset, step_rows, 0),
            lax.dynamic_slice_in_dim(value_rows, offset, step_rows, 0),
        )

    return lax.fori_loop(0, row_count // step_rows, one_block, state)


def empty_state(queries):
    state_shape = queries.shape[:3]
    return (
        jnp.full(state_shape, -1e30, jnp.float32),
        jnp.zeros(state_shape, jnp.float32),
        jnp.zeros(queries.shape, jnp.float32),
    )


def finish(state):
    largest, weight_sum, accumulated = state
    merged = accumulated / weight_sum[..., None]
    return merged.reshape(merged.shape[0], -1).astype(jnp.bfloat16)


def on_device(
    queries_small,
    keys_small,
    values_small,
    queries_large,
    keys_large,
    values_large,
    query_gain_small,
    key_gain_small,
    query_gain_large,
    key_gain_large,
    residual_in,
    out_weight_small,
    out_weight_large,
    norm_gain,
    routes,
    route_scores,
    expert_gate,
    expert_up,
    expert_down,
):
    token_rows = queries_small.shape[0]
    offset = lax.axis_index("sp") * token_rows
    tables_small = grid_tables(offset, token_rows, HS_SMALL)
    tables_large = grid_tables(offset, token_rows, HS_LARGE)
    kv_small = keys_small.shape[1] // HS_SMALL
    kv_large = keys_large.shape[1] // HS_LARGE
    asked_small = normed_turn(
        queries_small.reshape(token_rows, -1, HS_SMALL), query_gain_small, tables_small
    ).reshape(token_rows, kv_small, -1, HS_SMALL)
    asked_large = normed_turn(
        queries_large.reshape(token_rows, -1, HS_LARGE), query_gain_large, tables_large
    ).reshape(token_rows, kv_large, -1, HS_LARGE)
    turned_small = normed_turn(
        keys_small.reshape(token_rows, kv_small, HS_SMALL), key_gain_small, tables_small
    ).reshape(token_rows, -1)
    turned_large = normed_turn(
        keys_large.reshape(token_rows, kv_large, HS_LARGE), key_gain_large, tables_large
    ).reshape(token_rows, -1)
    key_small = lax.all_gather(turned_small, "sp", axis=0, tiled=True)
    value_small = lax.all_gather(values_small, "sp", axis=0, tiled=True)
    key_large = lax.all_gather(turned_large, "sp", axis=0, tiled=True)
    value_large = lax.all_gather(values_large, "sp", axis=0, tiled=True)
    state_small = attend_rows(empty_state(asked_small), asked_small, key_small, value_small)
    state_large = attend_rows(empty_state(asked_large), asked_large, key_large, value_large)
    heard_small = finish(state_small)
    heard_large = finish(state_large)
    projected = lax.psum_scatter(
        (
            jnp.dot(heard_small, out_weight_small, preferred_element_type=jnp.float32)
            + jnp.dot(heard_large, out_weight_large, preferred_element_type=jnp.float32)
        ).astype(jnp.bfloat16),
        "tp",
        scatter_dimension=0,
        tiled=True,
    ).astype(jnp.float32)
    attended = (residual_in.astype(jnp.float32) + projected).astype(jnp.bfloat16)
    widened = attended.astype(jnp.float32)
    normed = (
        widened
        * lax.rsqrt(jnp.mean(widened * widened, axis=-1, keepdims=True) + norm_eps)
        * norm_gain
    ).astype(jnp.bfloat16)
    local_rows = routes.shape[0]
    top_count = routes.shape[1]
    sp_count = lax.axis_size("sp")
    local_experts = expert_gate.shape[0]
    expert_count = local_experts * sp_count
    capacity = max(2, (2 * top_count * local_rows + expert_count - 1) // expert_count)
    flat_routes = routes.reshape(-1)
    member = (flat_routes[:, None] == jnp.arange(expert_count, dtype=jnp.int32)[None, :]).astype(
        jnp.int32
    )
    ranks = jnp.sum((jnp.cumsum(member, axis=0) - member) * member, axis=1)
    slots = flat_routes * capacity + ranks
    picker = (
        slots[:, None] == jnp.arange(expert_count * capacity, dtype=jnp.int32)[None, :]
    ).astype(jnp.bfloat16)
    placer = jnp.sum(picker.reshape(local_rows, top_count, -1), axis=1)
    outgoing = jnp.einsum("ts,td->sd", placer, normed, preferred_element_type=jnp.float32).astype(
        jnp.bfloat16
    )
    outgoing = outgoing.reshape(sp_count, local_experts, capacity, -1)
    everyone = lax.all_gather(
        lax.all_to_all(outgoing, "sp", split_axis=0, concat_axis=0, tiled=True),
        "tp",
        axis=0,
        tiled=True,
    )
    gate_out = jnp.einsum(
        "secd,edf->secf", everyone, expert_gate, preferred_element_type=jnp.float32
    )
    up_out = jnp.einsum("secd,edf->secf", everyone, expert_up, preferred_element_type=jnp.float32)
    active = (jax.nn.silu(gate_out) * up_out).astype(jnp.bfloat16)
    summed = lax.psum_scatter(
        jnp.einsum(
            "secf,efd->secd", active, expert_down, preferred_element_type=jnp.float32
        ).astype(jnp.bfloat16),
        "tp",
        scatter_dimension=0,
        tiled=True,
    )
    returned = lax.all_to_all(summed, "sp", split_axis=0, concat_axis=0, tiled=True)
    back_rows = returned.reshape(expert_count * capacity, -1)
    chosen_rows = jnp.dot(picker, back_rows, preferred_element_type=jnp.float32).reshape(
        local_rows, top_count, -1
    )
    shares = route_scores / jnp.sum(route_scores, axis=1, keepdims=True)
    mixed = jnp.sum(chosen_rows * shares[:, :, None], axis=1)
    return (attended.astype(jnp.float32) + mixed).astype(jnp.bfloat16)


def solution(mesh):
    in_specs = (
        P(("grp", "sp"), "tp"),
        P(("grp", "sp"), "tp"),
        P(("grp", "sp"), "tp"),
        P(("grp", "sp"), "tp"),
        P(("grp", "sp"), "tp"),
        P(("grp", "sp"), "tp"),
        P("grp"),
        P("grp"),
        P("grp"),
        P("grp"),
        P(("grp", "sp", "tp"), None),
        P("tp", None),
        P("tp", None),
        P(),
        P(("grp", "sp", "tp"), None),
        P(("grp", "sp", "tp"), None),
        P("sp", None, "tp"),
        P("sp", None, "tp"),
        P("sp", "tp", None),
    )
    out_specs = P(("grp", "sp", "tp"), None)
    return jax.shard_map(
        on_device, mesh=mesh, in_specs=in_specs, out_specs=out_specs, check_vma=False
    )
```

profile of v0, /device:TPU:0, one launch (start us, length us, event | category | flops | bytes accessed | tf_op | source)
XLA Modules:
  0.0 313.0 jit_solution(7394251430156797041)
XLA Ops:
  6.6 1.1 copy.83
  9.8 15.7 %all_gather.17 = bf16[1024,128]{0,1:T(8,128)(2,1)S(1)} all-gather(bf16[256,128]{0,1:T(8,128)(2,1)S(1)} %pad_maximum_fusion.1), channel_id=1, replica_groups=mesh['grp'=2,'sp'=4,'tp'=4] {'sp'}, dimensions={0}, use_global_device_ids=true | all-gather | bytes 327680 | tf_op jit(solution)/shard_map/all_gather | solution.py:160
  27.8 1.3 copy-done.2
  29.5 14.4 %all_gather.18 = bf16[1024,128]{0,1:T(8,128)(2,1)S(1)} all-gather(bf16[256,128]{0,1:T(8,128)(2,1)S(1)} %copy.87), channel_id=1, replica_groups=mesh['grp'=2,'sp'=4,'tp'=4] {'sp'}, dimensions={0}, use_global_device_ids=true | all-gather | bytes 327680 | tf_op jit(solution)/shard_map/all_gather | solution.py:161
  44.5 13.8 %all_gather.15 = bf16[1024,128]{0,1:T(8,128)(2,1)S(1)} all-gather(bf16[256,128]{0,1:T(8,128)(2,1)S(1)} %bitcast.168), channel_id=1, replica_groups=mesh['grp'=2,'sp'=4,'tp'=4] {'sp'}, dimensions={0}, use_global_device_ids=true | all-gather | bytes 327680 | tf_op jit(solution)/shard_map/all_gather | solution.py:158
  60.1 1.2 copy-done.1
  61.3 13.8 %all_gather.16 = bf16[1024,128]{1,0:T(8,128)(2,1)S(1)} all-gather(bf16[256,128]{1,0:T(8,128)(2,1)S(1)} %copy-done.8), channel_id=1, replica_groups=mesh['grp'=2,'sp'=4,'tp'=4] {'sp'}, dimensions={0}, use_global_device_ids=true | all-gather | bytes 327680 | tf_op jit(solution)/shard_map/all_gather | solution.py:159
  75.3 3.1 fusion.38
  78.9 1.1 copy-done.3
  80.5 1.5 fusion.3
  83.1 25.4 %reduce-scatter.5.cloned.1.call-done = bf16[64,2048]{1,0:T(8,128)(2,1)} async-done(((bf16[256,2048]{1,0:T(8,128)(2,1)}), bf16[64,2048]{1,0:T(8,128)(2,1)}) %reduce-scatter.5.cloned.1.call-update) | async-done | bytes 262160 | tf_op jit(solution)/shard_map/reduce_scatter | solution.py:166
  108.5 1.1 fusion.48
  109.7 1.4 convolution_convert_fusion
  111.1 30.0 %all_to_all.10 = bf16[4,2,32,2048]{3,2,1,0:T(8,128)(2,1)S(1)} all-to-all(bf16[4,2,32,2048]{3,2,1,0:T(8,128)(2,1)S(1)} %bitcast.163), channel_id=1, replica_groups=mesh['grp'=2,'sp'=4,'tp'=4] {'sp'}, dimensions={0} | all-to-all | bytes 2097152 | tf_op jit(solution)/shard_map/all_to_all | solution.py:203
  141.1 1.0 copy.91
  142.4 32.5 %all-gather.2.cloned.1.call-done = bf16[16,2,32,2048]{3,2,0,1:T(8,128)(2,1)} async-done(((bf16[4,2,32,2048]{3,2,0,1:T(8,128)(2,1)}), bf16[16,2,32,2048]{3,2,0,1:T(8,128)(2,1)}) %all-gather.2.cloned.1.call-update) | async-done | bytes 4194320 | tf_op jit(solution)/shard_map/all_gather | solution.py:202
  174.9 4.1 %fusion.14 = f32[16,2,32,256]{3,2,0,1:T(8,128)S(1)} fusion(bf16[16,2,32,2048]{3,2,0,1:T(8,128)(2,1)} %all-gather.2.cloned.1.call-done, bf16[2,2048,256]{2,1,0:T(8,128)(2,1)} %param.35), kind=kOutput, calls=%fused_computation.21 | convolution fusion | flops 1073741824 | bytes 7340032 | tf_op jit(solution)/shard_map/secd,edf->secf/dot_general | solution.py:208
  179.0 7.3 %convert_bitcast_fusion = bf16[16,2,32,2048]{3,2,0,1:T(8,128)(2,1)} fusion(bf16[2,256,2048]{2,1,0:T(8,128)(2,1)S(1)} %copy-done, bf16[16,2,32,2048]{3,2,0,1:T(8,128)(2,1)} %all-gather.2.cloned.1.call-done, bf16[2,2048,256]{2,1,0:T(8,128)(2,1)} %param.36, f32[16,2,32,256]{3,2,0,1:T(8,128)S(1)} %fusion.14), kind=kOutput, calls=%fused_computation.3 | convolution fusion | flops 2151153664 | bytes 13631488 | tf_op jit(solution)/shard_map/secf,efd->secd/dot_general | solution.py:214
  188.2 83.8 %all-reduce.3.cloned.1.call-done = bf16[16,2,32,2048]{3,2,0,1:T(8,128)(2,1)} async-done(((bf16[16,2,32,2048]{3,2,0,1:T(8,128)(2,1)}), bf16[16,2,32,2048]{3,2,0,1:T(8,128)(2,1)}) %all-reduce.3.cloned.1.call-update) | async-done | bytes 4194320
  272.0 1.3 constant_dynamic-slice_fusion
  273.3 1.1 copy.92
  274.4 4.6 %all-to-all-start.1 = ((bf16[4,2,32,2048]{3,2,1,0:T(8,128)(2,1)}), bf16[4,2,32,2048]{3,2,1,0:T(8,128)(2,1)S(1)}, u32[]{:S(2)}, u32[]{:S(2)}) async-start(bf16[4,2,32,2048]{3,2,1,0:T(8,128)(2,1)} %copy.92), calls=%async_computation.2 | async-start | bytes 2097152 | tf_op jit(solution)/shard_map/all_to_all | solution.py:221
  279.0 25.4 %all-to-all-done.1 = bf16[4,2,32,2048]{3,2,1,0:T(8,128)(2,1)S(1)} async-done(((bf16[4,2,32,2048]{3,2,1,0:T(8,128)(2,1)}), bf16[4,2,32,2048]{3,2,1,0:T(8,128)(2,1)S(1)}, u32[]{:S(2)}, u32[]{:S(2)}) %all-to-all-start.1) | async-done | bytes 1048608 | tf_op jit(solution)/shard_map/all_to_all | solution.py:221
  304.7 1.7 fusion.51
  (92 shorter events, 11.1 us)
Async XLA Ops:
  6.5 172.5 %copy-start = (bf16[2,256,2048]{2,1,0:T(8,128)(2,1)S(1)}, bf16[2,256,2048]{2,1,0:T(8,128)(2,1)}, u32[]{:S(2)}) copy-start(bf16[2,256,2048]{2,1,0:T(8,128)(2,1)} %param.37) | copy-start | bytes 6291460
  6.5 20.1 %copy-start.14 = (f32[128]{0:T(128)S(1)}, f32[128]{0:T(128)}, u32[]{:S(2)}) copy-start(f32[128]{0:T(128)} %param.27) | copy-start | bytes 1540
  6.5 102.0 %reduce-scatter.5.cloned.1.call-start = ((), (), s32[]{:S(2)}) async-start(), calls=%async_computation.3 | async-start | bytes 1310720 | tf_op jit(solution)/shard_map/reduce_scatter | solution.py:166
  27.1 2.4 copy-start.9
  27.1 17.1 %copy-start.10 = (bf16[256,128]{1,0:T(8,128)(2,1)S(1)}, bf16[256,128]{1,0:T(8,128)(2,1)}, u32[]{:S(2)}) copy-start(bf16[256,128]{1,0:T(8,128)(2,1)} %param.20) | copy-start | bytes 196612
  27.7 1.3 copy-start.2
  27.7 16.6 %copy-start.15 = (f32[64]{0:T(128)S(1)}, f32[64]{0:T(128)}, u32[]{:S(2)}) copy-start(f32[64]{0:T(128)} %param.26) | copy-start | bytes 772
  27.7 30.6 %copy-start.7 = (bf16[256,256]{1,0:T(8,128)(2,1)S(1)}, bf16[256,256]{1,0:T(8,128)(2,1)}, u32[]{:S(2)}) copy-start(bf16[256,256]{1,0:T(8,128)(2,1)} %param.19) | copy-start | bytes 393220
  27.7 30.7 %copy-start.16 = (f32[64]{0:T(128)S(1)}, f32[64]{0:T(128)}, u32[]{:S(2)}) copy-start(f32[64]{0:T(128)} %param.25) | copy-start | bytes 772
  59.4 1.9 copy-start.1
  59.4 1.9 copy-start.8
  75.3 3.1 copy-start.5
  78.4 1.6 copy-start.3
  78.9 1.6 copy-start.6
  80.5 1.6 copy-start.12
  80.5 28.0 %copy-start.4 = (bf16[64,2048]{1,0:T(8,128)(2,1)S(1)}, bf16[64,2048]{1,0:T(8,128)(2,1)}, u32[]{:S(2)}) copy-start(bf16[64,2048]{1,0:T(8,128)(2,1)} %param.29) | copy-start | bytes 786436
  80.5 29.1 %copy-start.11 = (f32[2048]{0:T(1024)S(1)}, f32[2048]{0:T(1024)}, u32[]{:S(2)}) copy-start(f32[2048]{0:T(1024)} %param.32) | copy-start | bytes 24580
  82.0 92.9 %all-gather.2.cloned.1.call-start = ((), (), s32[]{:S(2)}) async-start(), calls=%async_computation.4 | async-start | bytes 5242880 | tf_op jit(solution)/shard_map/all_gather | solution.py:202
  142.1 129.9 %all-reduce.3.cloned.1.call-start = ((), (), s32[]{:S(2)}) async-start(), calls=%async_computation.5 | async-start | bytes 8388608
  186.3 0.7 copy-start.17
  273.3 5.7 %copy-start.13 = (f32[64,2]{0,1:T(2,128)S(1)}, f32[64,2]{0,1:T(2,128)}, u32[]{:S(2)}) copy-start(f32[64,2]{0,1:T(2,128)} %param.34) | copy-start | bytes 1540
  274.4 30.0 %all-to-all-start.1 = ((bf16[4,2,32,2048]{3,2,1,0:T(8,128)(2,1)}), bf16[4,2,32,2048]{3,2,1,0:T(8,128)(2,1)S(1)}, u32[]{:S(2)}, u32[]{:S(2)}) async-start(bf16[4,2,32,2048]{3,2,1,0:T(8,128)(2,1)} %copy.92), calls=%async_computation.2 | async-start | bytes 2097152 | tf_op jit(solution)/shard_map/all_to_all | solution.py:221
Sparse Core Ops, SparseCore 0:
  82.1 26.3 reduce-scatter.4
  142.3 32.5 all-gather.1
  186.5 85.4 all-reduce.2
where the time goes:
time: 313 us
  waiting for transfers between devices  167 us (53%)
  blocking collectives  87.7 us (28%)
  matrix products  20.1 us (6%)
  between operations  14.3 us (5%)
  local copies, waits for them, and re-layouts  11.3 us (4%)
  other arithmetic  7.66 us (2%)
  starting transfers between devices  4.86 us (2%)
    unnamed x4, waiting for transfers between devices  83.8 us
    all_gather x1, waiting for transfers between devices, on_device(): lax.all_gather(lax.all_to_all(outgoing, 'sp', split_axis=0, concat_axis=0...  32.5 us
    all_to_all x1, blocking collectives, on_device(): lax.all_to_all(outgoing, 'sp', split_axis=0, concat_axis=0, tiled=True)  30 us
    reduce_scatter x1, waiting for transfers between devices, on_device(): lax.psum_scatter((jnp.dot(heard_small, out_weight_small, preferred_elemen...  25.4 us
    all_to_all x1, waiting for transfers between devices, on_device(): lax.all_to_all(summed, 'sp', split_axis=0, concat_axis=0, tiled=True)  25.4 us
    all_gather x1, blocking collectives, on_device(): key_large = lax.all_gather(turned_large, 'sp', axis=0, tiled=True)  15.7 us
    all_gather x1, blocking collectives, on_device(): value_large = lax.all_gather(values_large, 'sp', axis=0, tiled=True)  14.4 us
    all_gather x1, blocking collectives, on_device(): key_small = lax.all_gather(turned_small, 'sp', axis=0, tiled=True)  13.8 us
  transfers between devices with their start and end apart: 4, of which 4 were waited for; matrix products, arithmetic and copies ran while one was open for 1% of the time, Pallas kernels for 0%

commit v1 on v0

--- a/solution.py
+++ b/solution.py
@@ -157,7 +157,12 @@
     ).reshape(token_rows, -1)
     key_small = lax.all_gather(turned_small, "sp", axis=0, tiled=True)
     value_small = lax.all_gather(values_small, "sp", axis=0, tiled=True)
-    key_large = lax.all_gather(turned_large, "sp", axis=0, tiled=True)
+    ring = [turned_large]
+    for hop in range(3):
+        ring.append(lax.ppermute(ring[-1], "sp", [(dev, (dev + 1) % 4) for dev in range(4)]))
+    key_large = jnp.roll(
+        jnp.concatenate(ring[::-1], axis=0), (lax.axis_index("sp") + 1) * ring[0].shape[0], axis=0
+    )
     value_large = lax.all_gather(values_large, "sp", axis=0, tiled=True)
     state_small = attend_rows(empty_state(asked_small), asked_small, key_small, value_small)
     state_large = attend_rows(empty_state(asked_large), asked_large, key_large, value_large)

time: 313 us -> 309 us (0.987)
  blocking collectives: 87.7 us -> 71.9 us
  waiting for transfers between devices: 167 us -> 172 us
  starting transfers between devices: 4.86 us -> 8.03 us
    all_gather x1 -> x0, blocking collectives: 15.7 us -> none  [on_device(): key_large = lax.all_gather(turned_large, 'sp', axis=0, tiled=True)]
    ppermute x0 -> x3, waiting for transfers between devices: none -> 5.35 us  [on_device(): lax.ppermute(ring[-1], 'sp', [(dev, (dev + 1) % 4) for dev in range(4)])]
    ppermute x0 -> x3, starting transfers between devices: none -> 3.17 us  [on_device(): lax.ppermute(ring[-1], 'sp', [(dev, (dev + 1) % 4) for dev in range(4)])]
  transfers between devices with their start and end apart: 4 -> 7, of which waited for: 4 -> 5; matrix products, arithmetic and copies ran while one was open for 1% -> 4% of each run, Pallas kernels for 0% -> 0%
where the time goes in v1:
time: 309 us; the launch traced here: 308 us
  waiting for transfers between devices  172 us (56%)
  blocking collectives  71.9 us (23%)
  matrix products  21.4 us (7%)
  between operations  14.3 us (5%)
  local copies, waits for them, and re-layouts  11.1 us (4%)
  other arithmetic  8.95 us (3%)
  starting transfers between devices  8.03 us (3%)
    unnamed x4, waiting for transfers between devices  83.8 us
    all_gather x1, waiting for transfers between devices, on_device(): lax.all_gather(lax.all_to_all(outgoing, 'sp', split_axis=0, concat_axis=0...  32.5 us
    all_to_all x1, blocking collectives, on_device(): lax.all_to_all(outgoing, 'sp', split_axis=0, concat_axis=0, tiled=True)  30 us
    all_to_all x1, waiting for transfers between devices, on_device(): lax.all_to_all(summed, 'sp', split_axis=0, concat_axis=0, tiled=True)  25.4 us
    reduce_scatter x1, waiting for transfers between devices, on_device(): lax.psum_scatter((jnp.dot(heard_small, out_weight_small, preferred_elemen...  25.3 us
    all_gather x1, blocking collectives, on_device(): key_small = lax.all_gather(turned_small, 'sp', axis=0, tiled=True)  14.2 us
    all_gather x1, blocking collectives, on_device(): value_large = lax.all_gather(values_large, 'sp', axis=0, tiled=True)  14 us
    all_gather x1, blocking collectives, on_device(): value_small = lax.all_gather(values_small, 'sp', axis=0, tiled=True)  13.8 us
  transfers between devices with their start and end apart: 7, of which 5 were waited for; matrix products, arithmetic and copies ran while one was open for 4% of the time, Pallas kernels for 0%

profile of v1, /device:TPU:0, one launch (start us, length us, event | category | flops | bytes accessed | tf_op | source)
XLA Modules:
  0.0 308.1 jit_solution(8811530244078643748)
XLA Ops:
  6.6 1.1 copy.83
  9.4 3.1 collective-permute-start
  15.2 14.2 %all_gather.12 = bf16[1024,128]{0,1:T(8,128)(2,1)S(1)} all-gather(bf16[256,128]{0,1:T(8,128)(2,1)S(1)} %bitcast.168), channel_id=1, replica_groups=mesh['grp'=2,'sp'=4,'tp'=4] {'sp'}, dimensions={0}, use_global_device_ids=true | all-gather | bytes 327680 | tf_op jit(solution)/shard_map/all_gather | solution.py:158
  32.7 1.2 copy-done.1
  33.9 13.8 %all_gather.13 = bf16[1024,128]{1,0:T(8,128)(2,1)S(1)} all-gather(bf16[256,128]{1,0:T(8,128)(2,1)S(1)} %copy-done.6), channel_id=1, replica_groups=mesh['grp'=2,'sp'=4,'tp'=4] {'sp'}, dimensions={0}, use_global_device_ids=true | all-gather | bytes 327680 | tf_op jit(solution)/shard_map/all_gather | solution.py:159
  47.9 3.1 %fusion.38 = bf16[256,2,2,64]{0,3,2,1:T(8,128)(2,1)S(1)} fusion(bf16[1024,2,64,1]{0,2,3,1:T(8,128)(2,1)S(1)} %bitcast.166, f32[2,1024,256,2]{2,1,3,0:T(8,128)} %copy-done.1, f32[256,2,2]{0,2,1:T(2,128)S(1)} %broadcast_maximum_fusion, f32[256,2,2]{0,2,1:T(2,128)S(1)} %get-tuple-element.30, f32[256,2,2]{0,2,1:T(2,128)S(1)} %get-tuple-element.29), kind=kOutput, calls=%fused_computation.32 | convolution fusion | flops 137560064 | bytes 4599808 | tf_op jit(solution)/shard_map/qgrk,kgd->qgrd/dot_general | solution.py:77
  51.0 1.8 fusion.119
  53.8 5.3 %collective-permute-done.1 = bf16[256,128]{0,1:T(8,128)(2,1)S(1)} collective-permute-done((bf16[256,128]{0,1:T(8,128)(2,1)S(1)}, bf16[256,128]{0,1:T(8,128)(2,1)S(1)}, u32[]{:S(2)}, u32[]{:S(2)}) %collective-permute-start.1) | collective-permute-done | bytes 65568 | tf_op jit(solution)/shard_map/ppermute | solution.py:162
  59.1 14.0 %all_gather.14 = bf16[1024,128]{0,1:T(8,128)(2,1)S(1)} all-gather(bf16[256,128]{0,1:T(8,128)(2,1)S(1)} %copy.87), channel_id=1, replica_groups=mesh['grp'=2,'sp'=4,'tp'=4] {'sp'}, dimensions={0}, use_global_device_ids=true | all-gather | bytes 327680 | tf_op jit(solution)/shard_map/all_gather | solution.py:166
  75.7 1.5 fusion.3
  78.3 25.3 %reduce-scatter.5.cloned.1.call-done = bf16[64,2048]{1,0:T(8,128)(2,1)} async-done(((bf16[256,2048]{1,0:T(8,128)(2,1)}), bf16[64,2048]{1,0:T(8,128)(2,1)}) %reduce-scatter.5.cloned.1.call-update) | async-done | bytes 262160 | tf_op jit(solution)/shard_map/reduce_scatter | solution.py:171
  103.6 1.1 fusion.48
  104.7 1.4 convolution_convert_fusion
  106.2 30.0 %all_to_all.10 = bf16[4,2,32,2048]{3,2,1,0:T(8,128)(2,1)S(1)} all-to-all(bf16[4,2,32,2048]{3,2,1,0:T(8,128)(2,1)S(1)} %bitcast.163), channel_id=1, replica_groups=mesh['grp'=2,'sp'=4,'tp'=4] {'sp'}, dimensions={0} | all-to-all | bytes 2097152 | tf_op jit(solution)/shard_map/all_to_all | solution.py:208
  136.1 1.0 copy.91
  137.4 32.5 %all-gather.2.cloned.1.call-done = bf16[16,2,32,2048]{3,2,0,1:T(8,128)(2,1)} async-done(((bf16[4,2,32,2048]{3,2,0,1:T(8,128)(2,1)}), bf16[16,2,32,2048]{3,2,0,1:T(8,128)(2,1)}) %all-gather.2.cloned.1.call-update) | async-done | bytes 4194320 | tf_op jit(solution)/shard_map/all_gather | solution.py:207
  170.0 4.1 %fusion.14 = f32[16,2,32,256]{3,2,0,1:T(8,128)S(1)} fusion(bf16[16,2,32,2048]{3,2,0,1:T(8,128)(2,1)} %all-gather.2.cloned.1.call-done, bf16[2,2048,256]{2,1,0:T(8,128)(2,1)} %param.35), kind=kOutput, calls=%fused_computation.21 | convolution fusion | flops 1073741824 | bytes 7340032 | tf_op jit(solution)/shard_map/secd,edf->secf/dot_general | solution.py:213
  174.1 7.3 %convert_bitcast_fusion = bf16[16,2,32,2048]{3,2,0,1:T(8,128)(2,1)} fusion(bf16[2,256,2048]{2,1,0:T(8,128)(2,1)S(1)} %copy-done, bf16[16,2,32,2048]{3,2,0,1:T(8,128)(2,1)} %all-gather.2.cloned.1.call-done, bf16[2,2048,256]{2,1,0:T(8,128)(2,1)} %param.36, f32[16,2,32,256]{3,2,0,1:T(8,128)S(1)} %fusion.14), kind=kOutput, calls=%fused_computation.3 | convolution fusion | flops 2151153664 | bytes 13631488 | tf_op jit(solution)/shard_map/secf,efd->secd/dot_general | solution.py:219
  183.3 83.8 %all-reduce.3.cloned.1.call-done = bf16[16,2,32,2048]{3,2,0,1:T(8,128)(2,1)} async-done(((bf16[16,2,32,2048]{3,2,0,1:T(8,128)(2,1)}), bf16[16,2,32,2048]{3,2,0,1:T(8,128)(2,1)}) %all-reduce.3.cloned.1.call-update) | async-done | bytes 4194320
  267.1 1.3 constant_dynamic-slice_fusion
  268.4 1.1 copy.92
  269.4 4.6 %all-to-all-start.1 = ((bf16[4,2,32,2048]{3,2,1,0:T(8,128)(2,1)}), bf16[4,2,32,2048]{3,2,1,0:T(8,128)(2,1)S(1)}, u32[]{:S(2)}, u32[]{:S(2)}) async-start(bf16[4,2,32,2048]{3,2,1,0:T(8,128)(2,1)} %copy.92), calls=%async_computation.2 | async-start | bytes 2097152 | tf_op jit(solution)/shard_map/all_to_all | solution.py:226
  274.1 25.4 %all-to-all-done.1 = bf16[4,2,32,2048]{3,2,1,0:T(8,128)(2,1)S(1)} async-done(((bf16[4,2,32,2048]{3,2,1,0:T(8,128)(2,1)}), bf16[4,2,32,2048]{3,2,1,0:T(8,128)(2,1)S(1)}, u32[]{:S(2)}, u32[]{:S(2)}) %all-to-all-start.1) | async-done | bytes 1048608 | tf_op jit(solution)/shard_map/all_to_all | solution.py:226
  299.8 1.7 fusion.51
  (99 shorter events, 14.2 us)
Async XLA Ops:
  6.5 167.5 %copy-start = (bf16[2,256,2048]{2,1,0:T(8,128)(2,1)S(1)}, bf16[2,256,2048]{2,1,0:T(8,128)(2,1)}, u32[]{:S(2)}) copy-start(bf16[2,256,2048]{2,1,0:T(8,128)(2,1)} %param.37) | copy-start | bytes 6291460
  6.5 8.3 %copy-start.7 = (bf16[256,128]{1,0:T(8,128)(2,1)S(1)}, bf16[256,128]{1,0:T(8,128)(2,1)}, u32[]{:S(2)}) copy-start(bf16[256,128]{1,0:T(8,128)(2,1)} %param.20) | copy-start | bytes 196612
  6.5 8.5 %copy-start.12 = (f32[64]{0:T(128)S(1)}, f32[64]{0:T(128)}, u32[]{:S(2)}) copy-start(f32[64]{0:T(128)} %param.26) | copy-start | bytes 772
  6.5 97.0 %reduce-scatter.5.cloned.1.call-start = ((), (), s32[]{:S(2)}) async-start(), calls=%async_computation.3 | async-start | bytes 1310720 | tf_op jit(solution)/shard_map/reduce_scatter | solution.py:171
  9.4 43.5 %collective-permute-start = (bf16[256,128]{0,1:T(8,128)(2,1)}, bf16[256,128]{0,1:T(8,128)(2,1)S(1)}, u32[]{:S(2)}, u32[]{:S(2)}) collective-permute-start(bf16[256,128]{0,1:T(8,128)(2,1)} %pad_maximum_fusion.1), channel_id=1, source_target_pairs={{0,4},{4,8},{8,12},{12,0},{1,5},{5,9},{9,13},{13,1},{2,6},{6,10},{... | collective-permute-start | bytes 196616 | tf_op jit(solution)/shard_map/ppermute | solution.py:162
  32.0 1.9 copy-start.1
  32.0 1.9 copy-start.6
  47.9 3.1 %copy-start.4 = (bf16[256,2048]{1,0:T(8,128)(2,1)S(1)}, bf16[256,2048]{1,0:T(8,128)(2,1)}, u32[]{:S(2)}) copy-start(bf16[256,2048]{1,0:T(8,128)(2,1)} %param.30) | copy-start | bytes 3145732
  51.0 1.8 copy-start.13
  52.8 0.8 copy-start.8
  53.0 6.2 %collective-permute-start.1 = (bf16[256,128]{0,1:T(8,128)(2,1)S(1)}, bf16[256,128]{0,1:T(8,128)(2,1)S(1)}, u32[]{:S(2)}, u32[]{:S(2)}) collective-permute-start(bf16[256,128]{0,1:T(8,128)(2,1)S(1)} %collective-permute-done), channel_id=1, source_target_pairs={{0,4},{4,8},{8,12},{12,0},{1,5},{5,9},{9,13},{13,1},{2,6},{6,10},{... | collective-permute-start | bytes 196616 | tf_op jit(solution)/shard_map/ppermute | solution.py:162
  59.1 14.0 %collective-permute-start.2 = (bf16[256,128]{0,1:T(8,128)(2,1)S(1)}, bf16[256,128]{0,1:T(8,128)(2,1)S(1)}, u32[]{:S(2)}, u32[]{:S(2)}) collective-permute-start(bf16[256,128]{0,1:T(8,128)(2,1)S(1)} %collective-permute-done.1), channel_id=1, source_target_pairs={{0,4},{4,8},{8,12},{12,0},{1,5},{5,9},{9,13},{13,1},{2,6},{6,10},{... | collective-permute-start | bytes 196616 | tf_op jit(solution)/shard_map/ppermute | solution.py:162
  73.9 1.6 copy-start.2
  73.9 1.8 copy-start.5
  75.7 1.5 copy-start.10
  75.7 27.9 %copy-start.3 = (bf16[64,2048]{1,0:T(8,128)(2,1)S(1)}, bf16[64,2048]{1,0:T(8,128)(2,1)}, u32[]{:S(2)}) copy-start(bf16[64,2048]{1,0:T(8,128)(2,1)} %param.29) | copy-start | bytes 786436
  75.7 29.0 %copy-start.9 = (f32[2048]{0:T(1024)S(1)}, f32[2048]{0:T(1024)}, u32[]{:S(2)}) copy-start(f32[2048]{0:T(1024)} %param.32) | copy-start | bytes 24580
  77.2 92.8 %all-gather.2.cloned.1.call-start = ((), (), s32[]{:S(2)}) async-start(), calls=%async_computation.4 | async-start | bytes 5242880 | tf_op jit(solution)/shard_map/all_gather | solution.py:207
  137.2 129.9 %all-reduce.3.cloned.1.call-start = ((), (), s32[]{:S(2)}) async-start(), calls=%async_computation.5 | async-start | bytes 8388608
  181.4 0.7 copy-start.14
  268.4 5.7 %copy-start.11 = (f32[64,2]{0,1:T(2,128)S(1)}, f32[64,2]{0,1:T(2,128)}, u32[]{:S(2)}) copy-start(f32[64,2]{0,1:T(2,128)} %param.34) | copy-start | bytes 1540
  269.4 30.0 %all-to-all-start.1 = ((bf16[4,2,32,2048]{3,2,1,0:T(8,128)(2,1)}), bf16[4,2,32,2048]{3,2,1,0:T(8,128)(2,1)S(1)}, u32[]{:S(2)}, u32[]{:S(2)}) async-start(bf16[4,2,32,2048]{3,2,1,0:T(8,128)(2,1)} %copy.92), calls=%async_computation.2 | async-start | bytes 2097152 | tf_op jit(solution)/shard_map/all_to_all | solution.py:226
Sparse Core Ops, SparseCore 0:
  77.3 26.2 reduce-scatter.4
  137.3 32.5 all-gather.1
  181.5 85.4 all-reduce.2
